TPU v7x, 32 devices: a whole 2x2x4 slice. The times are simulated.
32 devices in a mesh: grp: 2 (over y), sp: 4 (over z), tp: 4 (over x, core).
Axes of the slice: x: 2, y: 2, z: 4, core: 2. Of those that a mesh axis runs over, the one named last changes fastest.
Arguments:
- query_rows: bfloat16 [4096, 1024], P(('grp', 'sp'), 'tp'), parts along dimension 0, may hold values from -128 to 128
- key_rows: bfloat16 [4096, 256], P(('grp', 'sp'), 'tp'), parts along dimension 0, may hold values from -4 to 4
- value_rows: bfloat16 [4096, 256], P(('grp', 'sp'), 'tp'), parts along dimension 0, may hold values from -6 to 6
- sink_logits: float32 [16], P('tp'), may hold values from 3 to 7
- residual: bfloat16 [4096, 2048], P(('grp', 'sp', 'tp')), parts along dimension 0, may hold values from -6 to 6
- out_weight: bfloat16 [1024, 2048], P('tp'), may hold values from -0.1875 to 0.1875
- norm_gain: float32 [2048], replicated, may hold values from 0.1 to 1.9
- gate_weight: bfloat16 [16, 2048, 512], P(('sp', 'tp')), may hold values from -0.125 to 0.125
- up_weight: bfloat16 [16, 2048, 512], P(('sp', 'tp')), may hold values from -0.125 to 0.125
- down_weight: bfloat16 [16, 512, 2048], P(('sp', 'tp')), may hold values from -0.25 to 0.25
- routes: int32 [4096, 2], P(('grp', 'sp', 'tp')), parts along dimension 0, may hold values from 0 to 15, as said below
- route_weight: float32 [4096, 2], P(('grp', 'sp', 'tp')), parts along dimension 0, may hold values from 0.1 to 1
Outputs:
- layer_out: bfloat16 [4096, 2048], P(('grp', 'sp', 'tp')), parts along dimension 0
There are 2 independent parts, one for each index of `grp`. A program takes and returns all parts, laid end to end along the dimension named above; an argument that names none is the same for every part. Nothing has to cross between parts.
Inputs may be any that keep to these rules, and one draw needn't show every extreme that they name: `routes`: A token's two experts differ and lie in the same group of 4 consecutive experts. Among the 128 tokens of one device (aligned blocks of 128 rows) no expert is named more than 32 times; in every block each expert of one group, the same group for all blocks, is named exactly 32 times.
All inputs are finite; a program needn't handle non-finite values.
Results may differ from a plain program's by a relative error of at most 0.013.
Values may be sent and summed in bfloat16 or wider, within the bound.
No kernel may reach another device: no remote copies, remote signals or barrier semaphores. Data moves between devices by JAX's collectives and lax.ppermute only.
A program may use at most 64 MiB of HBM per device.

v0:
```python
import jax
import jax.numpy as jnp
from jax import lax
from jax.sharding import PartitionSpec as P

HDIM = 64
WINDOW = 128
rope_base = 10000.0
norm_eps = 1e-06


def shifted(block, axis, distance):
    devices = range(lax.axis_size(axis))
    route = [(i - distance, i) for i in devices if i - distance in devices]
    return lax.ppermute(block, axis, route)


def rotate(rows, positions, heads):
    half_dim = HDIM // 2
    values = rows.astype(jnp.float32).reshape(rows.shape[0], heads, HDIM)
    inverse = rope_base ** (-jnp.arange(half_dim, dtype=jnp.float32) / half_dim)
    angles = positions.astype(jnp.float32)[:, None] * inverse[None, :]
    cosines = jnp.cos(angles)[:, None, :]
    sines = jnp.sin(angles)[:, None, :]
    lower = values[..., :half_dim]
    upper = values[..., half_dim:]
    turned = jnp.concatenate(
        [lower * cosines - upper * sines, upper * cosines + lower * sines], axis=-1
    )
    return turned.reshape(rows.shape[0], heads * HDIM).astype(jnp.bfloat16)


def per_device(
    query_rows,
    key_rows,
    value_rows,
    sink_logits,
    residual,
    out_weight,
    norm_gain,
    gate_weight,
    up_weight,
    down_weight,
    routes,
    route_weight,
):
    tok_count = query_rows.shape[0]
    head_local = query_rows.shape[1] // HDIM
    group_local = key_rows.shape[1] // HDIM
    repeat = head_local // group_local
    first_pos = lax.axis_index("sp") * tok_count
    positions = first_pos + jnp.arange(tok_count, dtype=jnp.int32)
    rot_q = rotate(query_rows, positions, head_local)
    rot_k = rotate(key_rows, positions, group_local)
    tails = jnp.stack([rot_k[tok_count - WINDOW :], value_rows[tok_count - WINDOW :]])
    earlier = shifted(tails, "sp", 1)
    blocks = tok_count // WINDOW
    q_blocks = rot_q.reshape(blocks, WINDOW, group_local, repeat, HDIM)
    k_blocks = rot_k.reshape(blocks, WINDOW, group_local, HDIM)
    v_blocks = value_rows.reshape(blocks, WINDOW, group_local, HDIM)
    k_prev = jnp.concatenate(
        [earlier[0].reshape(1, WINDOW, group_local, HDIM), k_blocks[:-1]], axis=0
    )
    v_prev = jnp.concatenate(
        [earlier[1].reshape(1, WINDOW, group_local, HDIM), v_blocks[:-1]], axis=0
    )
    k_wide = jnp.concatenate([k_prev, k_blocks], axis=1)
    v_wide = jnp.concatenate([v_prev, v_blocks], axis=1)
    query_pos = jnp.arange(WINDOW) + WINDOW
    key_pos = jnp.arange(2 * WINDOW)
    distance = query_pos[:, None] - key_pos[None, :]
    in_band = (distance >= 0) & (distance < WINDOW)
    key_global = (
        first_pos + jnp.arange(blocks)[:, None, None] * WINDOW + key_pos[None, None, :] - WINDOW
    )
    allowed = in_band[None] & (key_global >= 0)
    scores = jnp.einsum(
        "nqgrd,nkgd->grnqk", q_blocks, k_wide, preferred_element_type=jnp.float32
    ) * HDIM ** (-0.5)
    scores = jnp.where(allowed[None, None], scores, -jnp.inf)
    sink_here = sink_logits.reshape(group_local, repeat)[:, :, None, None, None]
    largest = jnp.maximum(scores.max(axis=-1, keepdims=True), sink_here)
    exp_scores = jnp.exp(scores - largest)
    denominator = exp_scores.sum(axis=-1, keepdims=True) + jnp.exp(sink_here - largest)
    probs = (exp_scores / denominator).astype(jnp.bfloat16)
    attended = jnp.einsum("grnqk,nkgd->nqgrd", probs, v_wide, preferred_element_type=jnp.float32)
    attended = attended.astype(jnp.bfloat16).reshape(tok_count, head_local * HDIM)
    row_count = residual.shape[0]
    token_rows = lax.all_to_all(attended, "tp", split_axis=0, concat_axis=1, tiled=True)
    projected = jnp.dot(
        token_rows,
        lax.all_gather(out_weight, "tp", axis=0, tiled=True),
        preferred_element_type=jnp.float32,
    )
    stream_f = (residual.astype(jnp.float32) + projected).astype(jnp.bfloat16).astype(jnp.float32)
    normed = (
        stream_f
        * lax.rsqrt(jnp.mean(stream_f * stream_f, axis=-1, keepdims=True) + norm_eps)
        * norm_gain[None, :]
    ).astype(jnp.bfloat16)
    sp_count = lax.axis_size("sp")
    tp_count = lax.axis_size("tp")
    expert_count = sp_count * tp_count
    capacity = 4 * row_count // expert_count
    width = normed.shape[1]
    flat_expert = routes.reshape(-1)
    one_hot = (flat_expert[:, None] == jnp.arange(expert_count, dtype=jnp.int32)[None, :]).astype(
        jnp.int32
    )
    slot_rank = jnp.sum((jnp.cumsum(one_hot, axis=0) - one_hot) * one_hot, axis=1)
    slot_index = flat_expert * capacity + slot_rank
    token_of = jnp.arange(2 * row_count, dtype=jnp.int32) // 2
    outgoing = (
        jnp.zeros((expert_count * capacity, width), jnp.bfloat16)
        .at[slot_index]
        .set(normed[token_of])
    )
    outgoing = outgoing.reshape(expert_count, capacity, width)
    arrived = lax.all_to_all(outgoing, ("sp", "tp"), split_axis=0, concat_axis=0, tiled=True)
    flat_rows = arrived.reshape(-1, width)
    gate_out = jnp.dot(flat_rows, gate_weight[0], preferred_element_type=jnp.float32)
    up_out = jnp.dot(flat_rows, up_weight[0], preferred_element_type=jnp.float32)
    hidden = (jax.nn.silu(gate_out) * up_out).astype(jnp.bfloat16)
    produced = jnp.dot(hidden, down_weight[0], preferred_element_type=jnp.float32).astype(
        jnp.bfloat16
    )
    returned = lax.all_to_all(
        produced.reshape(arrived.shape), ("sp", "tp"), split_axis=0, concat_axis=0, tiled=True
    )
    gathered = returned.reshape(expert_count * capacity, width)[slot_index].astype(jnp.float32)
    weighted = gathered * route_weight.reshape(-1)[:, None]
    combined = weighted.reshape(row_count, 2, width).sum(axis=1)
    return (stream_f + combined).astype(jnp.bfloat16)


def solution(mesh):
    in_specs = (
        P(("grp", "sp"), "tp"),
        P(("grp", "sp"), "tp"),
        P(("grp", "sp"), "tp"),
        P("tp"),
        P(("grp", "sp", "tp"), None),
        P("tp", None),
        P(),
        P(("sp", "tp"), None, None),
        P(("sp", "tp"), None, None),
        P(("sp", "tp"), None, None),
        P(("grp", "sp", "tp"), None),
        P(("grp", "sp", "tp"), None),
    )
    out_specs = P(("grp", "sp", "tp"), None)
    return jax.shard_map(
        per_device, mesh=mesh, in_specs=in_specs, out_specs=out_specs, check_vma=False
    )
```

profile of v0, /device:TPU:11, one launch (start us, length us, event | category | flops | bytes accessed | tf_op | source)
XLA Modules:
  0.0 195.3 jit_solution(5464959872850920019)
XLA Ops:
  6.5 0.7 all-gather.2.cloned.1.call-update
  7.3 0.9 bitcast_convert_fusion
  8.2 0.3 fusion.38
  8.5 0.7 slice_bitcast_fusion.4
  9.3 3.2 %collective-permute-start = (bf16[2,128,64]{1,2,0:T(8,128)(2,1)S(1)}, bf16[2,128,64]{1,2,0:T(8,128)(2,1)S(1)}, u32[]{:S(2)}, u32[]{:S(2)}) collective-permute-start(bf16[2,128,64]{1,2,0:T(8,128)(2,1)S(1)} %pad_maximum_fusion), channel_id=1, source_target_pairs={{0,4},{4,8},{8,12},{1,5},{5,9},{9,13},{2,6},{6,10},{10,14},{3,7},{... | collective-permute-start | bytes 98312 | tf_op jit(solution)/shard_map/ppermute | solution.py:15
  12.5 0.8 copy.25
  13.4 0.1 eq.25
  13.5 0.1 copy.21
  13.8 0.6 reduce-window.6
  14.3 0.2 slice_reduce_fusion
  14.8 0.3 multiply_cosine_fusion
  15.2 0.2 broadcast_and_fusion
  15.7 0.1 mul.180
  15.9 0.5 fusion.47
  16.5 0.3 fusion.7
  16.9 1.2 convolution_convert_fusion.1
  18.1 4.5 %all-to-all-start = ((bf16[4,128,256]{1,2,0:T(8,128)(2,1)}), bf16[4,128,256]{1,2,0:T(8,128)(2,1)S(1)}, u32[]{:S(2)}, u32[]{:S(2)}) async-start(bf16[4,128,256]{1,2,0:T(8,128)(2,1)} %bitcast.20), calls=%async_computation | async-start | bytes 524288 | tf_op jit(solution)/shard_map/all_to_all | solution.py:89
  22.5 7.4 %all-to-all-done = bf16[4,128,256]{1,2,0:T(8,128)(2,1)S(1)} async-done(((bf16[4,128,256]{1,2,0:T(8,128)(2,1)}), bf16[4,128,256]{1,2,0:T(8,128)(2,1)S(1)}, u32[]{:S(2)}, u32[]{:S(2)}) %all-to-all-start) | async-done | bytes 262176 | tf_op jit(solution)/shard_map/all_to_all | solution.py:89
  29.9 16.9 %all-gather.2.cloned.1.call-done = bf16[1024,2048]{1,0:T(8,128)(2,1)} async-done(((bf16[256,2048]{1,0:T(8,128)(2,1)}), bf16[1024,2048]{1,0:T(8,128)(2,1)}) %all-gather.2.cloned.1.call-update) | async-done | bytes 4194320 | tf_op jit(solution)/shard_map/all_gather | solution.py:92
  46.9 3.1 %multiply_reduce_fusion.1 = (f32[128]{0:T(128)S(1)}, f32[128,2048]{1,0:T(8,128)S(1)}) fusion(bf16[128,1024]{0,1:T(8,128)(2,1)S(1)} %bitcast.116, bf16[1024,2048]{1,0:T(8,128)(2,1)} %all-gather.2.cloned.1.call-done, bf16[128,2048]{1,0:T(8,128)(2,1)} %param.16), kind=kOutput, calls=%fused_computation.25 | convolution fusion | flops 538443648 | bytes 6029824 | tf_op jit(solution)/shard_map/dot_general | solution.py:90
  50.0 1.0 multiply_convert_fusion
  51.0 7.3 %scatter_custom_fusion = bf16[512,2048]{1,0:T(8,128)(2,1)} fusion(s32[256]{0:T(256)S(1)} %bitcast.119, bf16[128,2048]{1,0:T(8,128)(2,1)} %multiply_convert_fusion, s32[1024]{0:T(1024)S(1)} %pad_clamp_fusion.1, bf16[]{:T(256)} %constant.56.clone.1), kind=kCustom, calls=%fused_computation.21 | custom fusion | bytes 2097664 | tf_op jit(solution)/shard_map/scatter | solution.py:116
  58.3 53.3 %all_to_all.29 = bf16[16,32,2048]{2,1,0:T(8,128)(2,1)S(1)} all-to-all(bf16[16,32,2048]{2,1,0:T(8,128)(2,1)} %bitcast.112), channel_id=1, replica_groups=mesh['grp'=2,'sp'=4,'tp'=4] {'sp','tp'}, dimensions={0} | all-to-all | bytes 4194304 | tf_op jit(solution)/shard_map/all_to_all | solution.py:119
  111.7 1.3 copy-done.1
  112.9 2.2 %fusion.5 = f32[512,512]{1,0:T(8,128)} fusion(bf16[512,2048]{1,0:T(8,128)(2,1)S(1)} %bitcast.114, bf16[1,2048,512]{2,1,0:T(8,128)(2,1)S(1)} %copy-done.8), kind=kOutput, calls=%fused_computation.11 | convolution fusion | flops 1073741824 | bytes 5242880 | tf_op jit(solution)/shard_map/dot_general | solution.py:121
  115.2 6.3 %convolution_convert_fusion = bf16[512,2048]{1,0:T(8,128)(2,1)} fusion(bf16[1,512,2048]{2,1,0:T(8,128)(2,1)S(1)} %copy-done, bf16[512,2048]{1,0:T(8,128)(2,1)} %bitcast.115, bf16[1,2048,512]{2,1,0:T(8,128)(2,1)} %param.20, f32[512,512]{1,0:T(8,128)} %fusion.5), kind=kOutput, calls=%fused_computation.3 | convolution fusion | flops 2150105088 | bytes 9437184 | tf_op jit(solution)/shard_map/dot_general | solution.py:124
  121.5 5.1 %all-to-all-start.2 = ((bf16[16,32,2048]{2,1,0:T(8,128)(2,1)}), bf16[16,32,2048]{2,1,0:T(8,128)(2,1)}, u32[]{:S(2)}, u32[]{:S(2)}) async-start(bf16[16,32,2048]{2,1,0:T(8,128)(2,1)} %bitcast.113), calls=%async_computation.2 | async-start | bytes 4194304 | tf_op jit(solution)/shard_map/all_to_all | solution.py:127
  126.7 47.4 %all-to-all-done.2 = bf16[16,32,2048]{2,1,0:T(8,128)(2,1)} async-done(((bf16[16,32,2048]{2,1,0:T(8,128)(2,1)}), bf16[16,32,2048]{2,1,0:T(8,128)(2,1)}, u32[]{:S(2)}, u32[]{:S(2)}) %all-to-all-start.2) | async-done | bytes 2097184 | tf_op jit(solution)/shard_map/all_to_all | solution.py:127
  174.1 5.2 %gather_fusion = bf16[256,2048]{1,0:T(8,128)(2,1)} fusion(bf16[512,2048]{1,0:T(8,128)(2,1)} %bitcast.33, s32[1024]{0:T(1024)S(1)} %pad_clamp_fusion), kind=kCustom, calls=%fused_computation.1 | custom fusion | bytes 2098176 | tf_op jit(solution)/shard_map/gather | solution.py:130
  179.3 3.4 %reshape.391 = f32[128,2,2048]{2,1,0:T(2,128)} reshape(bf16[256,2048]{1,0:T(8,128)(2,1)} %gather_fusion) | data formatting | bytes 3145728 | tf_op jit(solution)/shard_map/convert_element_type | solution.py:130
  182.7 4.8 %multiply_reduce_fusion = f32[128,2048]{1,0:T(8,128)S(1)} fusion(f32[128,2,2048]{2,1,0:T(2,128)} %reshape.391, f32[128,2]{1,0:T(8,128)S(1)} %copy.28), kind=kLoop, calls=%fused_computation.13 | loop fusion | flops 786432 | bytes 3146752 | tf_op jit(solution)/shard_map/reduce_sum | solution.py:132
  187.5 0.9 add_convert_fusion
  (54 shorter events, 1.1 us)
Async XLA Ops:
  6.5 108.6 %copy-start = (bf16[1,512,2048]{2,1,0:T(8,128)(2,1)S(1)}, bf16[1,512,2048]{2,1,0:T(8,128)(2,1)}, u32[]{:S(2)}) copy-start(bf16[1,512,2048]{2,1,0:T(8,128)(2,1)} %param.21) | copy-start | bytes 6291460
  6.5 8.2 %copy-start.5 = (s32[128,2]{0,1:T(2,128)S(1)}, s32[128,2]{0,1:T(2,128)}, u32[]{:S(2)}) copy-start(s32[128,2]{0,1:T(2,128)} %param.22) | copy-start | bytes 3076
  6.5 7.0 %copy-start.2 = (bf16[512,256]{1,0:T(8,128)(2,1)S(1)}, bf16[512,256]{1,0:T(8,128)(2,1)}, u32[]{:S(2)}) copy-start(bf16[512,256]{1,0:T(8,128)(2,1)} %param.12) | copy-start | bytes 786436
  6.5 40.3 %all-gather.2.cloned.1.call-start = ((), (), s32[]{:S(2)}) async-start(), calls=%async_computation.3 | async-start | bytes 5242880 | tf_op jit(solution)/shard_map/all_gather | solution.py:92
  7.3 8.2 %copy-start.3 = (bf16[512,64]{0,1:T(8,128)(2,1)S(1)}, bf16[512,64]{0,1:T(8,128)(2,1)}, u32[]{:S(2)}) copy-start(bf16[512,64]{0,1:T(8,128)(2,1)} %param.14) | copy-start | bytes 196612
  7.3 8.2 %slice-start = ((bf16[512,64]{0,1:T(8,128)(2,1)}), bf16[384,64]{0,1:T(8,128)(2,1)S(1)}, s32[]{:S(2)}) async-start(bf16[512,64]{0,1:T(8,128)(2,1)} %param.14), calls=%async_computation.4 | async-start | bytes 98304 | tf_op jit(solution)/shard_map/slice | solution.py:65
  9.3 6.6 %collective-permute-start = (bf16[2,128,64]{1,2,0:T(8,128)(2,1)S(1)}, bf16[2,128,64]{1,2,0:T(8,128)(2,1)S(1)}, u32[]{:S(2)}, u32[]{:S(2)}) collective-permute-start(bf16[2,128,64]{1,2,0:T(8,128)(2,1)S(1)} %pad_maximum_fusion), channel_id=1, source_target_pairs={{0,4},{4,8},{8,12},{1,5},{5,9},{9,13},{2,6},{6,10},{10,14},{3,7},{... | collective-permute-start | bytes 98312 | tf_op jit(solution)/shard_map/ppermute | solution.py:15
  15.5 0.9 copy-start.6
  18.1 11.8 %all-to-all-start = ((bf16[4,128,256]{1,2,0:T(8,128)(2,1)}), bf16[4,128,256]{1,2,0:T(8,128)(2,1)S(1)}, u32[]{:S(2)}, u32[]{:S(2)}) async-start(bf16[4,128,256]{1,2,0:T(8,128)(2,1)} %bitcast.20), calls=%async_computation | async-start | bytes 524288 | tf_op jit(solution)/shard_map/all_to_all | solution.py:89
  46.9 3.2 %copy-start.4 = (f32[2048]{0:T(1024)S(1)}, f32[2048]{0:T(1024)}, u32[]{:S(2)}) copy-start(f32[2048]{0:T(1024)} %param.18) | copy-start | bytes 24580
  58.3 54.6 %copy-start.8 = (bf16[1,2048,512]{2,1,0:T(8,128)(2,1)S(1)}, bf16[1,2048,512]{2,1,0:T(8,128)(2,1)}, u32[]{:S(2)}) copy-start(bf16[1,2048,512]{2,1,0:T(8,128)(2,1)} %param.19) | copy-start | bytes 6291460
  111.6 1.3 copy-start.1
  121.5 5.1 %copy-start.7 = (f32[128,2]{0,1:T(2,128)S(1)}, f32[128,2]{0,1:T(2,128)}, u32[]{:S(2)}) copy-start(f32[128,2]{0,1:T(2,128)} %param.23) | copy-start | bytes 3076
  121.5 52.7 %all-to-all-start.2 = ((bf16[16,32,2048]{2,1,0:T(8,128)(2,1)}), bf16[16,32,2048]{2,1,0:T(8,128)(2,1)}, u32[]{:S(2)}, u32[]{:S(2)}) async-start(bf16[16,32,2048]{2,1,0:T(8,128)(2,1)} %bitcast.113), calls=%async_computation.2 | async-start | bytes 4194304 | tf_op jit(solution)/shard_map/all_to_all | solution.py:127
Sparse Core Ops, SparseCore 0:
  8.9 37.9 all-gather.1
where the time goes:
time: 196 us; the launch traced here: 195 us
  waiting for transfers between devices  72.4 us (37%)
  blocking collectives  53.3 us (27%)
  local copies, waits for them, and re-layouts  19.8 us (10%)
  between operations  13.7 us (7%)
  matrix products  13.4 us (7%)
  starting transfers between devices  12.8 us (7%)
  other arithmetic  9.91 us (5%)
    all_to_all x1, blocking collectives, per_device(): lax.all_to_all(outgoing, ('sp', 'tp'), split_axis=0, concat_axis=0, tiled...  53.3 us
    all_to_all x1, waiting for transfers between devices, per_device(): lax.all_to_all(produced.reshape(arrived.shape), ('sp', 'tp'), split_axis=...  47.4 us
    all_gather x1, waiting for transfers between devices, per_device(): lax.all_gather(out_weight, 'tp', axis=0, tiled=True)  16.9 us
    all_to_all x1, waiting for transfers between devices, per_device(): lax.all_to_all(attended, 'tp', split_axis=0, concat_axis=1, tiled=True)  7.37 us
    scatter x1, local copies, waits for them, and re-layouts, per_device(): outgoing = jnp.zeros((expert_count * capacity, width), jnp.bfloat16).at[s...  7.33 us
    dot_general x1, matrix products, per_device(): jnp.dot(hidden, down_weight[0], preferred_element_type=jnp.float32)  6.28 us
    gather x1, local copies, waits for them, and re-layouts, per_device(): returned.reshape(expert_count * capacity, width)[slot_index]  5.2 us
    all_to_all x1, starting transfers between devices, per_device(): lax.all_to_all(produced.reshape(arrived.shape), ('sp', 'tp'), split_axis=...  5.14 us
  transfers between devices with their start and end apart: 4, of which 3 were waited for; matrix products, arithmetic and copies ran while one was open for 4% of the time, Pallas kernels for 0%

commit v1 on v0

--- a/solution.py
+++ b/solution.py
@@ -7,6 +7,11 @@
 WINDOW = 128
 rope_base = 10000.0
 norm_eps = 1e-06
+
+
+def exchange_gather(value, name, d):
+    sent = jnp.stack([value] * lax.axis_size(name))
+    return jnp.concatenate(lax.all_to_all(sent, name, 0, 0), axis=d)
 
 
 def shifted(block, axis, distance):
@@ -88,9 +93,7 @@
     row_count = residual.shape[0]
     token_rows = lax.all_to_all(attended, "tp", split_axis=0, concat_axis=1, tiled=True)
     projected = jnp.dot(
-        token_rows,
-        lax.all_gather(out_weight, "tp", axis=0, tiled=True),
-        preferred_element_type=jnp.float32,
+        token_rows, exchange_gather(out_weight, "tp", 0), preferred_element_type=jnp.float32
     )
     stream_f = (residual.astype(jnp.float32) + projected).astype(jnp.bfloat16).astype(jnp.float32)
     normed = (

time: 196 us -> 217 us (1.11)
  waiting for transfers between devices: 72.4 us -> 92.2 us
  between operations: 13.7 us -> 0.29 us
  blocking collectives: 53.3 us -> 62.9 us
  local copies, waits for them, and re-layouts: 19.8 us -> 23.5 us
  starting transfers between devices: 12.8 us -> 15.2 us
    all_to_all x1, waiting for transfers between devices: 7.37 us -> 44.8 us  [exchange_gather(): return jnp.concatenate(lax.all_to_all(sent, name, 0, 0), axis=d)]
    all_gather x1 -> x0, waiting for transfers between devices: 16.9 us -> none  [per_device(): lax.all_gather(out_weight, 'tp', axis=0, tiled=True)]
    all_to_all x0 -> x1, blocking collectives: none -> 8.84 us  [per_device(): lax.all_to_all(attended, 'tp', split_axis=0, concat_axis=1, tiled=True)]
    another operation x1 -> x2, local copies, waits for them, and re-layouts: 0.01 us -> 2.5 us  [the longest x1 2.49 us: exchange_gather(): sent = jnp.stack([value] * lax.axis_size(name))]
    all_to_all x1, starting transfers between devices: 4.47 us -> 6.81 us  [exchange_gather(): return jnp.concatenate(lax.all_to_all(sent, name, 0, 0), axis=d)]
  transfers between devices with their start and end apart: 4 -> 3, of which waited for: 3 -> 2; matrix products, arithmetic and copies ran while one was open for 4% -> 2% of each run, Pallas kernels for 0% -> 0%
where the time goes in v1:
time: 217 us
  waiting for transfers between devices  92.2 us (42%)
  blocking collectives  62.9 us (29%)
  local copies, waits for them, and re-layouts  23.5 us (11%)
  starting transfers between devices  15.2 us (7%)
  matrix products  12.6 us (6%)
  other arithmetic  10.1 us (5%)
    all_to_all x1, blocking collectives, per_device(): lax.all_to_all(outgoing, ('sp', 'tp'), split_axis=0, concat_axis=0, tiled...  54 us
    all_to_all x1, waiting for transfers between devices, per_device(): lax.all_to_all(produced.reshape(arrived.shape), ('sp', 'tp'), split_axis=...  47.4 us
    all_to_all x1, waiting for transfers between devices, exchange_gather(): return jnp.concatenate(lax.all_to_all(sent, name, 0, 0), axis=d)  44.8 us
    all_to_all x1, blocking collectives, per_device(): lax.all_to_all(attended, 'tp', split_axis=0, concat_axis=1, tiled=True)  8.84 us
    scatter x1, local copies, waits for them, and re-layouts, per_device(): outgoing = jnp.zeros((expert_count * capacity, width), jnp.bfloat16).at[s...  7.36 us
    all_to_all x1, starting transfers between devices, exchange_gather(): return jnp.concatenate(lax.all_to_all(sent, name, 0, 0), axis=d)  6.81 us
    dot_general x1, matrix products, per_device(): jnp.dot(hidden, down_weight[0], preferred_element_type=jnp.float32)  6.27 us
    gather x1, local copies, waits for them, and re-layouts, per_device(): returned.reshape(expert_count * capacity, width)[slot_index]  5.2 us
  transfers between devices with their start and end apart: 3, of which 2 were waited for; matrix products, arithmetic and copies ran while one was open for 2% of the time, Pallas kernels for 0%

profile of v1, /device:TPU:11, one launch (start us, length us, event | category | flops | bytes accessed | tf_op | source)
XLA Modules:
  0.0 216.7 jit_solution(2857090912306702190)
XLA Ops:
  0.0 1.0 bitcast_convert_fusion
  1.1 0.7 slice_bitcast_fusion.4
  1.8 0.3 fusion.40
  2.1 3.2 %collective-permute-start = (bf16[2,128,64]{1,2,0:T(8,128)(2,1)S(1)}, bf16[2,128,64]{1,2,0:T(8,128)(2,1)S(1)}, u32[]{:S(2)}, u32[]{:S(2)}) collective-permute-start(bf16[2,128,64]{1,2,0:T(8,128)(2,1)S(1)} %pad_maximum_fusion), channel_id=1, source_target_pairs={{0,4},{4,8},{8,12},{1,5},{5,9},{9,13},{2,6},{6,10},{10,14},{3,7},{... | collective-permute-start | bytes 98312 | tf_op jit(solution)/shard_map/ppermute | solution.py:20
  5.4 0.3 multiply_cosine_fusion
  5.8 1.1 copy.22
  7.0 0.2 broadcast_and_fusion
  7.4 0.5 fusion.49
  8.0 0.3 fusion.8
  8.4 0.5 convolution_convert_fusion.1
  8.9 0.9 copy.25
  9.8 8.8 %all_to_all.31 = bf16[4,128,256]{2,1,0:T(8,128)(2,1)S(1)} all-to-all(bf16[4,128,256]{2,1,0:T(8,128)(2,1)} %copy.25), channel_id=1, replica_groups=mesh['grp'=2,'sp'=4,'tp'=4] {'tp'}, dimensions={0} | all-to-all | bytes 524288 | tf_op jit(solution)/shard_map/all_to_all | solution.py:94
  18.6 2.5 %stack.19 = bf16[4,256,2048]{2,1,0:T(8,128)(2,1)} broadcast(bf16[256,2048]{1,0:T(8,128)(2,1)S(1)} %copy-done.2), dimensions={1,2} | broadcast | bytes 5242880 | tf_op jit(solution)/shard_map/stack | solution.py:13
  21.1 6.8 %all-to-all-start.1 = ((bf16[4,256,2048]{2,1,0:T(8,128)(2,1)}), bf16[4,256,2048]{2,1,0:T(8,128)(2,1)}, u32[]{:S(2)}, u32[]{:S(2)}) async-start(bf16[4,256,2048]{2,1,0:T(8,128)(2,1)} %stack.19), calls=%async_computation.1 | async-start | bytes 8388608 | tf_op jit(solution)/shard_map/all_to_all | solution.py:14
  28.2 0.1 eq.29
  28.5 0.1 mul.180
  28.6 0.6 reduce-window.6
  29.2 0.2 slice_reduce_fusion
  29.6 44.8 %all-to-all-done.1 = bf16[4,256,2048]{2,1,0:T(8,128)(2,1)} async-done(((bf16[4,256,2048]{2,1,0:T(8,128)(2,1)}), bf16[4,256,2048]{2,1,0:T(8,128)(2,1)}, u32[]{:S(2)}, u32[]{:S(2)}) %all-to-all-start.1) | async-done | bytes 4194336 | tf_op jit(solution)/shard_map/all_to_all | solution.py:14
  74.3 3.1 %multiply_reduce_fusion.1 = (f32[128]{0:T(128)S(1)}, f32[128,2048]{1,0:T(8,128)S(1)}) fusion(bf16[4,256,2048]{2,1,0:T(8,128)(2,1)} %all-to-all-done.1, bf16[4,128,256]{2,1,0:T(8,128)(2,1)S(1)} %all_to_all.31, bf16[128,2048]{1,0:T(8,128)(2,1)} %param.16), kind=kOutput, calls=%fused_computation.26 | convolution fusion | flops 538443648 | bytes 6029824 | tf_op jit(solution)/shard_map/dot_general | solution.py:95
  77.5 0.9 multiply_convert_fusion
  78.5 7.4 %scatter_custom_fusion = bf16[512,2048]{1,0:T(8,128)(2,1)} fusion(s32[256]{0:T(256)S(1)} %bitcast.127, bf16[128,2048]{1,0:T(8,128)(2,1)} %multiply_convert_fusion, s32[1024]{0:T(1024)S(1)} %pad_clamp_fusion.1, bf16[]{:T(256)} %constant.56.clone.1), kind=kCustom, calls=%fused_computation.22 | custom fusion | bytes 2097664 | tf_op jit(solution)/shard_map/scatter | solution.py:119
  85.8 54.0 %all_to_all.32 = bf16[16,32,2048]{2,1,0:T(8,128)(2,1)S(1)} all-to-all(bf16[16,32,2048]{2,1,0:T(8,128)(2,1)} %bitcast.121), channel_id=1, replica_groups=mesh['grp'=2,'sp'=4,'tp'=4] {'sp','tp'}, dimensions={0} | all-to-all | bytes 4194304 | tf_op jit(solution)/shard_map/all_to_all | solution.py:122
  139.8 1.3 copy-done.1
  141.1 2.2 %fusion.6 = f32[512,512]{1,0:T(8,128)} fusion(bf16[512,2048]{1,0:T(8,128)(2,1)S(1)} %bitcast.123, bf16[1,2048,512]{2,1,0:T(8,128)(2,1)S(1)} %copy-done.8), kind=kOutput, calls=%fused_computation.12 | convolution fusion | flops 1073741824 | bytes 5242880 | tf_op jit(solution)/shard_map/dot_general | solution.py:124
  143.4 6.3 %convolution_convert_fusion = bf16[512,2048]{1,0:T(8,128)(2,1)} fusion(bf16[1,512,2048]{2,1,0:T(8,128)(2,1)S(1)} %copy-done, bf16[512,2048]{1,0:T(8,128)(2,1)} %bitcast.124, bf16[1,2048,512]{2,1,0:T(8,128)(2,1)} %param.20, f32[512,512]{1,0:T(8,128)} %fusion.6), kind=kOutput, calls=%fused_computation.3 | convolution fusion | flops 2150105088 | bytes 9437184 | tf_op jit(solution)/shard_map/dot_general | solution.py:127
  149.6 5.2 %all-to-all-start.3 = ((bf16[16,32,2048]{2,1,0:T(8,128)(2,1)}), bf16[16,32,2048]{2,1,0:T(8,128)(2,1)}, u32[]{:S(2)}, u32[]{:S(2)}) async-start(bf16[16,32,2048]{2,1,0:T(8,128)(2,1)} %bitcast.122), calls=%async_computation.3 | async-start | bytes 4194304 | tf_op jit(solution)/shard_map/all_to_all | solution.py:130
  154.9 47.4 %all-to-all-done.3 = bf16[16,32,2048]{2,1,0:T(8,128)(2,1)} async-done(((bf16[16,32,2048]{2,1,0:T(8,128)(2,1)}), bf16[16,32,2048]{2,1,0:T(8,128)(2,1)}, u32[]{:S(2)}, u32[]{:S(2)}) %all-to-all-start.3) | async-done | bytes 2097184 | tf_op jit(solution)/shard_map/all_to_all | solution.py:130
  202.3 5.2 %gather_fusion = bf16[256,2048]{1,0:T(8,128)(2,1)} fusion(bf16[512,2048]{1,0:T(8,128)(2,1)} %bitcast.33, s32[1024]{0:T(1024)S(1)} %pad_clamp_fusion), kind=kCustom, calls=%fused_computation.1 | custom fusion | bytes 2098176 | tf_op jit(solution)/shard_map/gather | solution.py:133
  207.5 3.4 %reshape.394 = f32[128,2,2048]{2,1,0:T(2,128)} reshape(bf16[256,2048]{1,0:T(8,128)(2,1)} %gather_fusion) | data formatting | bytes 3145728 | tf_op jit(solution)/shard_map/convert_element_type | solution.py:133
  210.9 4.8 %multiply_reduce_fusion = f32[128,2048]{1,0:T(8,128)S(1)} fusion(f32[128,2,2048]{2,1,0:T(2,128)} %reshape.394, f32[128,2]{1,0:T(8,128)S(1)} %copy.30), kind=kLoop, calls=%fused_computation.14 | loop fusion | flops 786432 | bytes 3146752 | tf_op jit(solution)/shard_map/reduce_sum | solution.py:135
  215.7 0.9 add_convert_fusion
  (54 shorter events, 1.2 us)
Async XLA Ops:
  0.0 143.4 %copy-start = (bf16[1,512,2048]{2,1,0:T(8,128)(2,1)S(1)}, bf16[1,512,2048]{2,1,0:T(8,128)(2,1)}, u32[]{:S(2)}) copy-start(bf16[1,512,2048]{2,1,0:T(8,128)(2,1)} %param.21) | copy-start | bytes 6291460
  0.0 7.3 %copy-start.3 = (bf16[512,64]{0,1:T(8,128)(2,1)S(1)}, bf16[512,64]{0,1:T(8,128)(2,1)}, u32[]{:S(2)}) copy-start(bf16[512,64]{0,1:T(8,128)(2,1)} %param.14) | copy-start | bytes 196612
  0.0 7.4 %slice-start = ((bf16[512,64]{0,1:T(8,128)(2,1)}), bf16[384,64]{0,1:T(8,128)(2,1)S(1)}, s32[]{:S(2)}) async-start(bf16[512,64]{0,1:T(8,128)(2,1)} %param.14), calls=%async_computation.4 | async-start | bytes 98304 | tf_op jit(solution)/shard_map/slice | solution.py:70
  2.1 5.3 %collective-permute-start = (bf16[2,128,64]{1,2,0:T(8,128)(2,1)S(1)}, bf16[2,128,64]{1,2,0:T(8,128)(2,1)S(1)}, u32[]{:S(2)}, u32[]{:S(2)}) collective-permute-start(bf16[2,128,64]{1,2,0:T(8,128)(2,1)S(1)} %pad_maximum_fusion), channel_id=1, source_target_pairs={{0,4},{4,8},{8,12},{1,5},{5,9},{9,13},{2,6},{6,10},{10,14},{3,7},{... | collective-permute-start | bytes 98312 | tf_op jit(solution)/shard_map/ppermute | solution.py:20
  7.3 0.7 copy-start.6
  8.4 10.2 %copy-start.2 = (bf16[256,2048]{1,0:T(8,128)(2,1)S(1)}, bf16[256,2048]{1,0:T(8,128)(2,1)}, u32[]{:S(2)}) copy-start(bf16[256,2048]{1,0:T(8,128)(2,1)} %param.17) | copy-start | bytes 3145732
  21.1 6.8 %copy-start.5 = (s32[128,2]{0,1:T(2,128)S(1)}, s32[128,2]{0,1:T(2,128)}, u32[]{:S(2)}) copy-start(s32[128,2]{0,1:T(2,128)} %param.22) | copy-start | bytes 3076
  21.1 53.2 %all-to-all-start.1 = ((bf16[4,256,2048]{2,1,0:T(8,128)(2,1)}), bf16[4,256,2048]{2,1,0:T(8,128)(2,1)}, u32[]{:S(2)}, u32[]{:S(2)}) async-start(bf16[4,256,2048]{2,1,0:T(8,128)(2,1)} %stack.19), calls=%async_computation.1 | async-start | bytes 8388608 | tf_op jit(solution)/shard_map/all_to_all | solution.py:14
  29.6 47.9 %copy-start.4 = (f32[2048]{0:T(1024)S(1)}, f32[2048]{0:T(1024)}, u32[]{:S(2)}) copy-start(f32[2048]{0:T(1024)} %param.18) | copy-start | bytes 24580
  85.8 55.3 %copy-start.8 = (bf16[1,2048,512]{2,1,0:T(8,128)(2,1)S(1)}, bf16[1,2048,512]{2,1,0:T(8,128)(2,1)}, u32[]{:S(2)}) copy-start(bf16[1,2048,512]{2,1,0:T(8,128)(2,1)} %param.19) | copy-start | bytes 6291460
  139.8 1.3 copy-start.1
  149.6 5.2 %copy-start.7 = (f32[128,2]{0,1:T(2,128)S(1)}, f32[128,2]{0,1:T(2,128)}, u32[]{:S(2)}) copy-start(f32[128,2]{0,1:T(2,128)} %param.23) | copy-start | bytes 3076
  149.6 52.7 %all-to-all-start.3 = ((bf16[16,32,2048]{2,1,0:T(8,128)(2,1)}), bf16[16,32,2048]{2,1,0:T(8,128)(2,1)}, u32[]{:S(2)}, u32[]{:S(2)}) async-start(bf16[16,32,2048]{2,1,0:T(8,128)(2,1)} %bitcast.122), calls=%async_computation.3 | async-start | bytes 4194304 | tf_op jit(solution)/shard_map/all_to_all | solution.py:130
